TPU v7x, 32 devices: a whole 2x2x4 slice. The times are simulated.
32 devices in a mesh: fs: 16 (over z, y, x), tp: 2 (over core).
Axes of the slice: x: 2, y: 2, z: 4, core: 2. Of those that a mesh axis runs over, the one named last changes fastest.
Arguments:
- block_input: bfloat16 [16384, 2048], P('fs'), may hold values from -6 to 6
- value_cotangent: bfloat16 [16384, 1024], P('fs', 'tp'), may hold values from -6 to 6
- mixed_output: bfloat16 [16384, 1024], P('fs', 'tp'), may hold values from -6 to 6
- output_cotangent: bfloat16 [16384, 2048], P('fs'), may hold values from -6 to 6
- value_weight: float32 [2048, 1024], P('fs', 'tp'), may hold values from -0.125 to 0.125
- output_weight: float32 [1024, 2048], P('tp', 'fs'), may hold values from -0.1875 to 0.1875
- value_basis: bfloat16 [2048, 384], P('fs'), may hold values from -0.125 to 0.125
- output_basis: bfloat16 [2048, 384], P('fs'), may hold values from -0.125 to 0.125
- value_mean: float32 [384, 1024], P(None, 'tp'), may hold values from -4 to 4
- value_square: float32 [384, 1024], P(None, 'tp'), may hold values from 0.3 to 2
- output_mean: float32 [1024, 384], P('tp'), may hold values from -4 to 4
- output_square: float32 [1024, 384], P('tp'), may hold values from 0.3 to 2
Outputs:
- value_next: float32 [2048, 1024], P('fs', 'tp')
- value_copy: bfloat16 [2048, 1024], P(None, 'tp')
- value_step: float32 [2048, 1024], P('fs', 'tp')
- value_mean_next: float32 [384, 1024], P(None, 'tp')
- value_square_next: float32 [384, 1024], P(None, 'tp')
- output_next: float32 [1024, 2048], P('tp', 'fs')
- output_copy: bfloat16 [1024, 2048], P('tp')
- output_step: float32 [1024, 2048], P('tp', 'fs')
- output_mean_next: float32 [1024, 384], P('tp')
- output_square_next: float32 [1024, 384], P('tp')
All inputs are finite; a program needn't handle non-finite values.
Results may differ from a plain program's by a relative error of at most 0.002.
Values may be sent and summed in bfloat16 or wider, within the bound.
A program may use at most 64 MiB of HBM per device.

v0:
```python
import math

import jax
import jax.numpy as jnp
from jax import lax
from jax.sharding import PartitionSpec as P


def split_product(wide_left, narrow_right, contract):
    leading = wide_left.astype(jnp.bfloat16)
    trailing = (wide_left - leading.astype(jnp.float32)).astype(jnp.bfloat16)
    first = lax.dot_general(leading, narrow_right, contract, preferred_element_type=jnp.float32)
    second = lax.dot_general(trailing, narrow_right, contract, preferred_element_type=jnp.float32)
    return first + second


def on_device(
    block_input,
    value_cotangent,
    mixed_output,
    output_cotangent,
    value_weight,
    output_weight,
    value_basis,
    output_basis,
    value_mean,
    value_square,
    output_mean,
    output_square,
):
    highest = lax.Precision.HIGHEST
    tokens_all = block_input.shape[0] * lax.axis_size("fs")
    scaling = 1.0 / math.sqrt(tokens_all)
    rank_size = value_basis.shape[1]
    local_width = value_cotangent.shape[1]
    contract = (((0,), (0,)), ((), ()))
    input_proj = jnp.dot(
        block_input,
        lax.all_gather(value_basis, "fs", axis=0, tiled=True),
        preferred_element_type=jnp.float32,
    )
    cotangent_proj = jnp.dot(
        output_cotangent,
        lax.all_gather(output_basis, "fs", axis=0, tiled=True),
        preferred_element_type=jnp.float32,
    )
    value_part = split_product(input_proj, value_cotangent, contract)
    output_part = split_product(cotangent_proj, mixed_output, contract).T
    value_low, output_low = lax.psum((value_part * scaling, output_part * scaling), "fs")
    value_squares, output_squares = lax.psum(
        (jnp.sum(value_low * value_low), jnp.sum(output_low * output_low)), "tp"
    )
    entries = 2.0 * rank_size * local_width * lax.axis_size("tp")
    clip_scale = 1.0 / jnp.sqrt(1.0 + (value_squares + output_squares) / entries)
    value_scaled = clip_scale * value_low
    output_scaled = clip_scale * output_low
    value_mean_next = 0.8 * value_mean + 0.2 * value_scaled
    output_mean_next = 0.8 * output_mean + 0.2 * output_scaled
    value_square_next = 0.9 * value_square + 0.1 * value_scaled * value_scaled
    output_square_next = 0.9 * output_square + 0.1 * output_scaled * output_scaled
    value_norm = value_mean_next / jnp.sqrt(value_square_next + 0.1)
    output_norm = output_mean_next / jnp.sqrt(output_square_next + 0.1)
    value_step = jnp.dot(value_basis.astype(jnp.float32), value_norm, precision=highest)
    output_step = jnp.dot(output_norm, output_basis.astype(jnp.float32).T, precision=highest)
    value_next = value_weight - 0.02 * value_step
    output_next = output_weight - 0.02 * output_step
    value_copy = lax.all_gather(value_next.astype(jnp.bfloat16), "fs", axis=0, tiled=True)
    output_copy = lax.all_gather(output_next.astype(jnp.bfloat16), "fs", axis=1, tiled=True)
    return (
        value_next,
        value_copy,
        value_step,
        value_mean_next,
        value_square_next,
        output_next,
        output_copy,
        output_step,
        output_mean_next,
        output_square_next,
    )


def solution(mesh):
    placed = (
        P("fs", None),
        P("fs", "tp"),
        P("fs", "tp"),
        P("fs", None),
        P("fs", "tp"),
        P("tp", "fs"),
        P("fs", None),
        P("fs", None),
        P(None, "tp"),
        P(None, "tp"),
        P("tp", None),
        P("tp", None),
    )
    return jax.shard_map(
        on_device,
        mesh=mesh,
        in_specs=placed,
        out_specs=(
            P("fs", "tp"),
            P(None, "tp"),
            P("fs", "tp"),
            P(None, "tp"),
            P(None, "tp"),
            P("tp", "fs"),
            P("tp", None),
            P("tp", "fs"),
            P("tp", None),
            P("tp", None),
        ),
        check_vma=False,
    )
```

profile of v0, /device:TPU:0, one launch (start us, length us, event | category | flops | bytes accessed | tf_op | source)
XLA Modules:
  0.0 406.3 jit_solution(13357692029135591817)
XLA Ops:
  7.2 0.0 copy-start
  7.2 0.0 all-gather.7.cloned.1.call-start
  7.2 0.7 all-gather.7.cloned.1.call-update
  7.9 0.0 all-gather.5.cloned.1.call-start
  8.0 0.7 all-gather.5.cloned.1.call-update
  8.7 0.0 all-reduce.3.cloned.1.call-start
  8.7 62.8 %all-gather.7.cloned.1.call-done = bf16[2048,384]{1,0:T(8,128)(2,1)} async-done(((bf16[128,384]{1,0:T(8,128)(2,1)}), bf16[2048,384]{1,0:T(8,128)(2,1)}) %all-gather.7.cloned.1.call-update) | async-done | bytes 1572880 | tf_op jit(solution)/shard_map/all_gather | solution.py:44
  71.5 5.0 %fusion.25 = f32[1024,384]{1,0:T(8,128)S(1)} fusion(bf16[1024,2048]{1,0:T(8,128)(2,1)} %param.15, bf16[2048,384]{1,0:T(8,128)(2,1)} %all-gather.7.cloned.1.call-done), kind=kOutput, calls=%fused_computation.38 | convolution fusion | flops 1610612736 | bytes 7340032 | tf_op jit(solution)/shard_map/dot_general | solution.py:42
  76.5 0.6 fusion.15
  77.1 1.5 fusion.2
  78.6 52.4 %all-gather.5.cloned.1.call-done = bf16[2048,384]{1,0:T(8,128)(2,1)} async-done(((bf16[128,384]{1,0:T(8,128)(2,1)}), bf16[2048,384]{1,0:T(8,128)(2,1)}) %all-gather.5.cloned.1.call-update) | async-done | bytes 1572880 | tf_op jit(solution)/shard_map/all_gather | solution.py:39
  131.0 5.0 %fusion.24 = f32[1024,384]{1,0:T(8,128)S(1)} fusion(bf16[1024,2048]{1,0:T(8,128)(2,1)} %param.12, bf16[2048,384]{1,0:T(8,128)(2,1)} %all-gather.5.cloned.1.call-done), kind=kOutput, calls=%fused_computation.37 | convolution fusion | flops 1610612736 | bytes 7340032 | tf_op jit(solution)/shard_map/dot_general | solution.py:37
  136.0 0.6 fusion.18
  136.6 1.5 fusion
  138.1 0.0 all-reduce.3.cloned.1.call-update
  138.1 0.0 copy-start.8
  138.1 0.0 all-gather.11.cloned.1.call-start
  138.2 1.0 copy-done.7
  139.2 0.3 copy.23
  139.5 115.1 %all-reduce.3.cloned.1.call-done = (f32[384,512]{1,0:T(8,128)}, f32[512,384]{0,1:T(8,128)}) async-done(((f32[384,512]{1,0:T(8,128)}, f32[512,384]{0,1:T(8,128)}), (f32[384,512]{1,0:T(8,128)}, f32[512,384]{0,1:T(8,128)})) %all-reduce.3.cloned.1.call-update) | async-done | bytes 1572880 | tf_op jit(solution)/shard_map/psum | solution.py:49
  254.6 1.9 multiply_reduce_fusion
  256.5 1.9 multiply_reduce_fusion.1
  259.7 0.0 copy-done.8
  259.8 1.1 copy.24
  260.9 3.0 psum.32
  264.5 0.0 copy-start.9
  264.6 0.0 copy-start.11
  264.6 1.7 fusion.4
  266.3 1.7 fusion.22
  268.0 0.0 all-gather.11.cloned.1.call-update
  268.0 0.0 all-gather.9.cloned.1.call-start
  268.1 1.8 copy.22
  269.9 1.7 fusion.3
  271.6 0.0 copy-start.3
  271.6 0.0 copy-start.4
  271.6 0.9 copy-done.3
  272.5 0.0 copy-done.10
  272.5 1.5 fusion.23
  274.0 0.0 copy-done.4
  274.0 0.0 all-gather.9.cloned.1.call-update
  274.0 1.1 copy.29
  275.2 1.1 copy.28
  276.3 0.8 copy.25
  277.2 0.8 copy.27
  278.0 52.3 %all-gather.11.cloned.1.call-done = bf16[512,2048]{1,0:T(8,128)(2,1)} async-done(((bf16[512,128]{1,0:T(8,128)(2,1)}), bf16[512,2048]{1,0:T(8,128)(2,1)}) %all-gather.11.cloned.1.call-update) | async-done | bytes 2097168 | tf_op jit(solution)/shard_map/all_gather | solution.py:68
  330.3 64.3 %all-gather.9.cloned.1.call-done = bf16[2048,512]{0,1:T(8,128)(2,1)} async-done(((bf16[128,512]{0,1:T(8,128)(2,1)}), bf16[2048,512]{0,1:T(8,128)(2,1)}) %all-gather.9.cloned.1.call-update) | async-done | bytes 2097168 | tf_op jit(solution)/shard_map/all_gather | solution.py:67
  394.5 3.9 copy.26
  398.5 1.3 copy.33
  (13 shorter events, 0.0 us)
Async XLA Ops:
  7.2 69.3 %copy-start = (bf16[1024,512]{1,0:T(8,128)(2,1)S(1)}, bf16[1024,512]{1,0:T(8,128)(2,1)}, u32[]{:S(2)}) copy-start(bf16[1024,512]{1,0:T(8,128)(2,1)} %param.14) | copy-start | bytes 3145732
  7.2 64.3 %all-gather.7.cloned.1.call-start = ((), (), s32[]{:S(2)}) async-start(), calls=%async_computation.1 | async-start | bytes 1671168 | tf_op jit(solution)/shard_map/all_gather | solution.py:44
  7.9 123.0 %all-gather.5.cloned.1.call-start = ((), (), s32[]{:S(2)}) async-start(), calls=%async_computation | async-start | bytes 1671168 | tf_op jit(solution)/shard_map/all_gather | solution.py:39
  8.7 245.9 %all-reduce.3.cloned.1.call-start = ((), (), s32[]{:S(2)}) async-start(), calls=%async_computation.4 | async-start | bytes 3145728 | tf_op jit(solution)/shard_map/psum | solution.py:49
  78.6 57.4 %copy-start.1 = (bf16[1024,512]{1,0:T(8,128)(2,1)S(1)}, bf16[1024,512]{1,0:T(8,128)(2,1)}, u32[]{:S(2)}) copy-start(bf16[1024,512]{1,0:T(8,128)(2,1)} %param.13) | copy-start | bytes 3145732
  138.1 1.1 copy-start.7
  138.1 121.6 %copy-start.8 = (f32[512,384]{1,0:T(8,128)S(1)}, f32[512,384]{1,0:T(8,128)}, u32[]{:S(2)}) copy-start(f32[512,384]{1,0:T(8,128)} %param.23) | copy-start | bytes 2359300
  138.1 192.1 %all-gather.11.cloned.1.call-start = ((), (), s32[]{:S(2)}) async-start(), calls=%async_computation.3 | async-start | bytes 2228224 | tf_op jit(solution)/shard_map/all_gather | solution.py:68
  264.5 1.7 copy-start.9
  264.6 1.7 copy-start.11
  266.3 3.6 copy-start.2
  268.0 126.5 %all-gather.9.cloned.1.call-start = ((), (), s32[]{:S(2)}) async-start(), calls=%async_computation.2 | async-start | bytes 2228224 | tf_op jit(solution)/shard_map/all_gather | solution.py:67
  269.9 2.6 copy-start.6
  269.9 2.6 copy-start.10
  271.6 0.9 copy-start.3
  271.6 2.4 copy-start.4
  330.3 68.2 %copy-start.5 = (bf16[512,2048]{1,0:T(8,128)(2,1)S(1)}, bf16[512,2048]{1,0:T(8,128)(2,1)}, u32[]{:S(2)}) copy-start(bf16[512,2048]{1,0:T(8,128)(2,1)} %all-gather.11.cloned.1.call-done) | copy-start | bytes 6291460
Sparse Core Ops, SparseCore 0:
  10.8 60.6 all-gather.6
  74.3 56.6 all-gather.4
  138.2 116.2 all-reduce.2
  268.2 62.0 all-gather.10
  333.4 61.1 all-gather.8
where the time goes:
time: 407 us; the launch traced here: 406 us
  waiting for transfers between devices  348 us (86%)
  matrix products  17.4 us (4%)
  between operations  15.9 us (4%)
  local copies, waits for them, and re-layouts  14.4 us (4%)
  other arithmetic  7.3 us (2%)
    psum x1, waiting for transfers between devices, on_device(): lax.psum((value_part * scaling, output_part * scaling), 'fs')  115 us
    all_gather x1, waiting for transfers between devices, on_device(): lax.all_gather(value_next.astype(jnp.bfloat16), 'fs', axis=0, tiled=True)  64.3 us
    all_gather x1, waiting for transfers between devices, on_device(): lax.all_gather(output_basis, 'fs', axis=0, tiled=True)  62.8 us
    all_gather x1, waiting for transfers between devices, on_device(): lax.all_gather(value_basis, 'fs', axis=0, tiled=True)  52.4 us
    all_gather x1, waiting for transfers between devices, on_device(): lax.all_gather(output_next.astype(jnp.bfloat16), 'fs', axis=1, tiled=True)  52.3 us
    unnamed x33, local copies, waits for them, and re-layouts  14.4 us
  transfers between devices with their start and end apart: 5, of which 5 were waited for; matrix products, arithmetic and copies ran while one was open for 4% of the time, Pallas kernels for 0%

commit v1 on v0

v1 whole, which is shorter than its diff:
```python
import functools
import math

import jax
import jax.numpy as jnp
from jax import lax
from jax.experimental import pallas as pl
from jax.experimental.pallas import tpu as pltpu
from jax.sharding import PartitionSpec as P

MESH = pl.DeviceIdType.MESH
VALUE_RATE = 125.0 / 0.125
OUTPUT_RATE = 125.0 / 0.1875
TOKEN_TILE = 256


def split_fs(n):
    inner = 2 if n % 2 == 0 else 1
    middle = 2 if n % (2 * inner) == 0 else 1
    return n // (inner * middle), middle, inner


class Place:
    def __init__(self, n):
        self.sizes = split_fs(n)
        self.me = lax.axis_index("fs")
        self.core = lax.axis_index("tp")
        self.par = lax.rem(self.core, 2)
        _, b, c = self.sizes
        self.z = self.me // (b * c)
        self.y = lax.rem(self.me // c, b)
        self.x = lax.rem(self.me, c)

    def at(self, dz, ds, dt, par=None):
        a, b, c = self.sizes
        par = self.par if par is None else par
        dy = ds * (1 - par) + dt * par
        dx = ds * par + dt * (1 - par)
        z = lax.rem(self.z + dz + a, a)
        y = lax.rem(self.y + dy, b)
        x = lax.rem(self.x + dx, c)
        return (z * b + y) * c + x


class Gather:
    def __init__(self, place, slots, send, recv):
        self.p, self.slots, self.send, self.recv = place, slots, send, recv
        self.a = place.sizes[0]
        self.started = []

    def copy(self, j, src, to, sid, rid):
        ref = self.slots[j](src)
        return pltpu.make_async_remote_copy(
            src_ref=ref, dst_ref=ref, send_sem=self.send.at[j, sid], recv_sem=self.recv.at[j, rid],
            device_id={"fs": to}, device_id_type=MESH)

    def rel(self, dz, ds, dt):
        return (dz * 2 + ds) * 2 + dt

    def go(self, j, src, to, sid, rid):
        c = self.copy(j, src, to, sid, rid)
        c.start()
        self.started.append(c)

    def arrive(self, dz, ds, dt):
        for j in range(len(self.slots)):
            src = self.p.at(-dz, ds, dt)
            self.copy(j, src, self.p.me, 0, self.rel(dz, ds, dt)).wait_recv()

    def to_s(self, dz):
        for j in range(len(self.slots)):
            self.go(j, self.p.at(-dz, 0, 0), self.p.at(0, 1, 0), self.a + dz, self.rel(dz, 1, 0))

    def to_t(self, dz, ds):
        for j in range(len(self.slots)):
            self.go(j, self.p.at(-dz, ds, 0), self.p.at(0, 0, 1), 2 * self.a + dz * 2 + ds, self.rel(dz, ds, 1))

    def begin(self):
        for dz in range(1, self.a):
            for j in range(len(self.slots)):
                self.go(j, self.p.me, self.p.at(dz, 0, 0), dz, self.rel(dz, 0, 0))
        self.to_s(0)
        self.to_t(0, 0)

    def stage_z(self, seen=lambda *k: None):
        for dz in range(1, self.a):
            self.arrive(dz, 0, 0)
            self.to_s(dz)
            self.to_t(dz, 0)
            seen(dz, 0, 0)

    def stage_s(self, seen=lambda *k: None):
        for dz in range(self.a):
            self.arrive(dz, 1, 0)
            self.to_t(dz, 1)
            seen(dz, 1, 0)

    def stage_t(self, seen=lambda *k: None):
        for dz in range(self.a):
            for ds in range(2):
                self.arrive(dz, ds, 1)
                seen(dz, ds, 1)

    def finish(self):
        for c in self.started:
            c.wait_send()


def exchange(n, scaling, x_hbm, v_hbm, m_hbm, o_hbm, vb_ref, ob_ref, vw_ref, ow_ref,
             bases, wv, wo, low_v, low_o,
             x_ref, v_ref, m_ref, o_ref, acc_v, acc_o, part_v, part_o, got_v, got_o,
             load_sem, own_sem, b_send, b_recv, c_send, c_recv, w_send, w_recv, l_send, l_recv, r_send, r_recv):
    p = Place(n)
    a = p.sizes[0]
    par, me = p.par, p.me
    loads = [pltpu.make_async_copy(s, d, load_sem.at[i]) for i, (s, d) in enumerate(
        ((x_hbm, x_ref), (v_hbm, v_ref), (o_hbm, o_ref), (m_hbm, m_ref)))]
    own = [pltpu.make_async_copy(s, d, own_sem.at[i]) for i, (s, d) in enumerate(
        ((vb_ref, bases.at[0, me]), (ob_ref, bases.at[1, me]), (vw_ref, wv.at[me]), (ow_ref, wo.at[me])))]
    for c in own + loads:
        c.start()
    partner = p.core + 1 - 2 * par
    barrier = pltpu.get_barrier_semaphore()
    peers = [p.at(dz, 0, 0) for dz in range(1, a)] + [p.at(0, 1, 0), p.at(0, 0, 1)]
    for to in peers:
        pl.semaphore_signal(barrier, inc=1, device_id={"fs": to}, device_id_type=MESH)
    pl.semaphore_signal(barrier, inc=1, device_id={"tp": partner}, device_id_type=MESH)
    pl.semaphore_wait(barrier, len(peers) + 1)
    for c in own:
        c.wait()

    crossed = []

    def cross(dz, ds, dt):
        k = (dz * 2 + ds) * 2 + dt
        ref = bases.at[par, p.at(-dz, ds, dt)]
        c = pltpu.make_async_remote_copy(
            src_ref=ref, dst_ref=ref, send_sem=c_send.at[k], recv_sem=c_recv.at[k],
            device_id={"tp": partner}, device_id_type=MESH)
        c.start()
        crossed.append(c)

    gb = Gather(p, [lambda i: bases.at[par, i]], b_send, b_recv)
    gb.begin()
    gb.stage_z(cross)
    gb.stage_s(cross)
    gb.stage_t(cross)
    gw = Gather(p, [lambda i: wv.at[i], lambda i: wo.at[i]], w_send, w_recv)
    gw.begin()
    for dz in range(a):
        for ds in range(2):
            for dt in range(2):
                k = (dz * 2 + ds) * 2 + dt
                if k:
                    ref = bases.at[1 - par, p.at(-dz, ds, dt, 1 - par)]
                    pltpu.make_async_remote_copy(
                        src_ref=ref, dst_ref=ref, send_sem=c_send.at[k], recv_sem=c_recv.at[k],
                        device_id={"tp": partner}, device_id_type=MESH).wait_recv()
    for c in loads:
        c.wait()

    depth, rank = bases.shape[2], bases.shape[3]
    tokens = x_ref.shape[0]
    tile = math.gcd(tokens, TOKEN_TILE)
    acc_v[...] = jnp.zeros_like(acc_v)
    acc_o[...] = jnp.zeros_like(acc_o)
    whole_v = bases[0].reshape(n * depth, rank)
    whole_o = bases[1].reshape(n * depth, rank)
    first = (((0,), (0,)), ((), ()))

    def halves(value):
        high = value.astype(jnp.bfloat16)
        return high, (value - high.astype(jnp.float32)).astype(jnp.bfloat16)

    @pl.loop(0, tokens // tile)
    def _(step):
        rows = pl.ds(pl.multiple_of(step * tile, tile), tile)
        cot = v_ref[rows, :]
        for half in halves(jnp.dot(x_ref[rows, :], whole_v, preferred_element_type=jnp.float32)):
            acc_v[...] += lax.dot_general(half, cot, first, preferred_element_type=jnp.float32)
        mixed = m_ref[rows, :]
        for half in halves(jnp.dot(o_ref[rows, :], whole_o, preferred_element_type=jnp.float32)):
            acc_o[...] += lax.dot_general(mixed, half, first, preferred_element_type=jnp.float32)

    parts, gots = (part_v, part_o), (got_v, got_o)
    for part, acc in ((part_v, acc_v), (part_o, acc_o)):
        high = part.shape[1]
        for i in range(n):
            part[i] = acc[i * high:(i + 1) * high, :] * scaling

    sent = []

    def hand(block, to, slot):
        for j in range(2):
            c = pltpu.make_async_remote_copy(
                src_ref=parts[j].at[block], dst_ref=gots[j].at[slot],
                send_sem=r_send.at[j, slot], recv_sem=r_recv.at[j, slot],
                device_id={"fs": to}, device_id_type=MESH)
            c.start()
            sent.append(c)

    def take(block, slot):
        for j in range(2):
            pltpu.make_async_remote_copy(
                src_ref=parts[j].at[block], dst_ref=gots[j].at[slot],
                send_sem=r_send.at[j, slot], recv_sem=r_recv.at[j, slot],
                device_id={"fs": me}, device_id_type=MESH).wait_recv()
            parts[j][block] += gots[j][slot]

    order = list(range(1, a)) + [0]
    for dz in order:
        for ds in (1, 0):
            hand(p.at(dz, ds, 1), p.at(0, 0, 1), dz * 2 + ds)
    for dz in order:
        take(p.at(dz, 1, 0), dz * 2 + 1)
        hand(p.at(dz, 1, 0), p.at(0, 1, 0), 2 * a + dz)
        take(p.at(dz, 0, 0), dz * 2)
    for dz in order:
        take(p.at(dz, 0, 0), 2 * a + dz)
        if dz:
            hand(p.at(dz, 0, 0), p.at(dz, 0, 0), 3 * a + dz)
    gw.stage_z()
    for dz in range(1, a):
        take(me, 3 * a + dz)
    low_v[me] = part_v[me]
    low_o[me] = part_o[me]
    gl = Gather(p, [lambda i: low_v.at[i], lambda i: low_o.at[i]], l_send, l_recv)
    gl.begin()
    gl.stage_z()
    gl.stage_s()
    gl.stage_t()
    gw.stage_s()
    gw.stage_t()
    for c in crossed + sent:
        c.wait_send()
    gb.finish()
    gw.finish()
    gl.finish()


def low_and_weights(block_input, value_cotangent, mixed_output, output_cotangent, value_basis, output_basis, vw_code, ow_code):
    n = lax.axis_size("fs")
    depth, rank = value_basis.shape
    tokens, width = value_cotangent.shape
    wide = block_input.shape[1]
    a = split_fs(n)[0]
    scaling = 1.0 / math.sqrt(tokens * n)
    f32, b16 = jnp.float32, jnp.bfloat16
    rv, ro = rank // n, width // n
    vmem = pl.BlockSpec(memory_space=pltpu.VMEM)
    hbm = pl.BlockSpec(memory_space=pl.ANY)
    dma = pltpu.SemaphoreType.DMA
    return pl.pallas_call(
        functools.partial(exchange, n, scaling),
        out_shape=(
            jax.ShapeDtypeStruct((2, n, depth, rank), b16),
            jax.ShapeDtypeStruct((n,) + vw_code.shape, vw_code.dtype),
            jax.ShapeDtypeStruct((n,) + ow_code.shape, ow_code.dtype),
            jax.ShapeDtypeStruct((n, rv, width), f32),
            jax.ShapeDtypeStruct((n, ro, rank), f32),
        ),
        in_specs=[hbm] * 4 + [vmem] * 4,
        out_specs=[vmem] * 5,
        scratch_shapes=[
            pltpu.VMEM((tokens, wide), b16), pltpu.VMEM((tokens, width), b16),
            pltpu.VMEM((tokens, width), b16), pltpu.VMEM((tokens, wide), b16),
            pltpu.VMEM((rank, width), f32), pltpu.VMEM((width, rank), f32),
            pltpu.VMEM((n, rv, width), f32), pltpu.VMEM((n, ro, rank), f32),
            pltpu.VMEM((4 * a, rv, width), f32), pltpu.VMEM((4 * a, ro, rank), f32),
            dma((4,)), dma((4,)),
            dma((1, 4 * a)), dma((1, 4 * a)), dma((4 * a,)), dma((4 * a,)),
            dma((2, 4 * a)), dma((2, 4 * a)), dma((2, 4 * a)), dma((2, 4 * a)), dma((2, 4 * a)), dma((2, 4 * a)),
        ],
        compiler_params=pltpu.CompilerParams(
            collective_id=0, has_side_effects=True, vmem_limit_bytes=60 * 1024 * 1024),
    )(block_input, value_cotangent, mixed_output, output_cotangent, value_basis, output_basis, vw_code, ow_code)


def stepped(norm, basis, flip):
    high = norm.astype(jnp.bfloat16)
    low = (norm - high.astype(jnp.float32)).astype(jnp.bfloat16)
    if flip:
        return sum(lax.dot_general(h, basis, (((1,), (1,)), ((), ())), preferred_element_type=jnp.float32) for h in (high, low))
    return sum(jnp.dot(basis, h, preferred_element_type=jnp.float32) for h in (high, low))


def on_device(
    block_input,
    value_cotangent,
    mixed_output,
    output_cotangent,
    value_weight,
    output_weight,
    value_basis,
    output_basis,
    value_mean,
    value_square,
    output_mean,
    output_square,
):
    rank_size = value_basis.shape[1]
    local_width = value_cotangent.shape[1]
    wide = block_input.shape[1]
    bases, wv, wo, value_low, output_low = low_and_weights(
        block_input, value_cotangent, mixed_output, output_cotangent, value_basis, output_basis,
        jnp.exp2(VALUE_RATE * value_weight).astype(jnp.bfloat16),
        jnp.exp2(OUTPUT_RATE * output_weight).astype(jnp.bfloat16))
    value_low = value_low.reshape(rank_size, local_width)
    output_low = output_low.reshape(local_width, rank_size)
    squares = lax.psum(jnp.sum(value_low * value_low) + jnp.sum(output_low * output_low), "tp")
    entries = 2.0 * rank_size * local_width * lax.axis_size("tp")
    clip_scale = 1.0 / jnp.sqrt(1.0 + squares / entries)
    value_scaled = clip_scale * value_low
    output_scaled = clip_scale * output_low
    value_mean_next = 0.8 * value_mean + 0.2 * value_scaled
    output_mean_next = 0.8 * output_mean + 0.2 * output_scaled
    value_square_next = 0.9 * value_square + 0.1 * value_scaled * value_scaled
    output_square_next = 0.9 * output_square + 0.1 * output_scaled * output_scaled
    value_norm = value_mean_next / jnp.sqrt(value_square_next + 0.1)
    output_norm = output_mean_next / jnp.sqrt(output_square_next + 0.1)
    value_step = stepped(value_norm, value_basis, False)
    output_step = stepped(output_norm, output_basis, True)
    value_next = value_weight - 0.02 * value_step
    output_next = output_weight - 0.02 * output_step
    value_all = stepped(value_norm, bases[0].reshape(wide, rank_size), False)
    output_all = stepped(output_norm, bases[1].reshape(wide, rank_size), True)
    value_old = jnp.log2(wv.reshape(wide, local_width).astype(jnp.float32)) * (1.0 / VALUE_RATE)
    value_copy = (value_old - 0.02 * value_all).astype(jnp.bfloat16)
    output_old = jnp.log2(wo.transpose(1, 0, 2).reshape(local_width, wide).astype(jnp.float32)) * (1.0 / OUTPUT_RATE)
    output_copy = (output_old - 0.02 * output_all).astype(jnp.bfloat16)
    return (
        value_next,
        value_copy,
        value_step,
        value_mean_next,
        value_square_next,
        output_next,
        output_copy,
        output_step,
        output_mean_next,
        output_square_next,
    )


def solution(mesh):
    placed = (
        P("fs", None),
        P("fs", "tp"),
        P("fs", "tp"),
        P("fs", None),
        P("fs", "tp"),
        P("tp", "fs"),
        P("fs", None),
        P("fs", None),
        P(None, "tp"),
        P(None, "tp"),
        P("tp", None),
        P("tp", None),
    )
    return jax.shard_map(
        on_device,
        mesh=mesh,
        in_specs=placed,
        out_specs=(
            P("fs", "tp"),
            P(None, "tp"),
            P("fs", "tp"),
            P(None, "tp"),
            P(None, "tp"),
            P("tp", "fs"),
            P("tp", None),
            P("tp", "fs"),
            P("tp", None),
            P("tp", None),
        ),
        check_vma=False,
    )
```

time: 407 us -> 154 us (0.38)
  waiting for transfers between devices: 348 us -> 0 us
  Pallas kernels: 0 us -> 102 us
  between operations: 15.9 us -> 2.81 us
  other arithmetic: 7.3 us -> 17 us
  matrix products: 17.4 us -> 12.6 us
    all_gather x4 -> x0, waiting for transfers between devices: 232 us -> none  [the longest x1 64.3 us: on_device(): lax.all_gather(value_next.astype(jnp.bfloat16), 'fs', axis=0, tiled=True)]
    psum x1 -> x0, waiting for transfers between devices: 115 us -> none  [on_device(): lax.psum((value_part * scaling, output_part * scaling), 'fs')]
    pallas_call x0 -> x1, Pallas kernels: none -> 102 us  [low_and_weights(): pl.pallas_call(functools.partial(exchange, n, scaling), out_shape=(jax.Sh...]
    mul x0 -> x2, local copies, waits for them, and re-layouts: none -> 10.8 us  [on_device(): jnp.log2(wo.transpose(1, 0, 2).reshape(local_width, wide).astype(jnp.floa...]
    unnamed x33 -> x23, local copies, waits for them, and re-layouts: 14.4 us -> 3.78 us
    convert_element_type x0 -> x4, other arithmetic: none -> 6.91 us  [the longest x2 3.61 us: stepped(): low = (norm - high.astype(jnp.float32)).astype(jnp.bfloat16)]
    mul x0 -> x4, other arithmetic: none -> 6.22 us  [the longest x1 2.55 us: on_device(): jnp.log2(wo.transpose(1, 0, 2).reshape(local_width, wide).astype(jnp.floa...]
    dot_general x8, matrix products: 17.4 us -> 12.6 us  [the longest x4 7.34 us: stepped(): lax.dot_general(h, basis, (((1,), (1,)), ((), ())), preferred_element_typ...]
  transfers between devices with their start and end apart: 5 -> 0, of which waited for: 5 -> 0; matrix products, arithmetic and copies ran while one was open for 4% -> 0% of each run, Pallas kernels for 0% -> 0%
where the time goes in v1:
time: 154 us; the launch traced here: 153 us
  Pallas kernels  102 us (66%)
  other arithmetic  17 us (11%)
  local copies, waits for them, and re-layouts  15.1 us (10%)
  matrix products  12.6 us (8%)
  blocking collectives  3.15 us (2%)
  between operations  2.81 us (2%)
    pallas_call x1, Pallas kernels, low_and_weights(): pl.pallas_call(functools.partial(exchange, n, scaling), out_shape=(jax.Sh...  102 us
    mul x2, local copies, waits for them, and re-layouts, on_device(): jnp.log2(wo.transpose(1, 0, 2).reshape(local_width, wide).astype(jnp.floa...  10.8 us
    dot_general x4, matrix products, stepped(): lax.dot_general(h, basis, (((1,), (1,)), ((), ())), preferred_element_typ...  7.34 us
    dot_general x4, matrix products, stepped(): jnp.dot(basis, h, preferred_element_type=jnp.float32)  5.28 us
    unnamed x23, local copies, waits for them, and re-layouts  3.78 us
    convert_element_type x2, other arithmetic, stepped(): low = (norm - high.astype(jnp.float32)).astype(jnp.bfloat16)  3.61 us
    psum x1, blocking collectives, on_device(): lax.psum(jnp.sum(value_low * value_low) + jnp.sum(output_low * output_low...  3.15 us

profile of v1, /device:TPU:0, one launch (start us, length us, event | category | flops | bytes accessed | tf_op | source)
XLA Modules:
  0.0 152.6 jit_solution(16598555450936839542)
XLA Ops:
  0.6 1.1 copy.25
  1.7 1.7 %exponential_convert_fusion.1.vw_ref = bf16[128,512]{1,0:T(8,128)(2,1)} fusion(f32[128,512]{1,0:T(8,128)} %param.16), kind=kLoop, calls=%fused_computation.27 | loop fusion | flops 131072 | bytes 393216 | tf_op jit(solution)/shard_map/convert_element_type | solution.py:306
  3.4 1.6 %exponential_convert_fusion.ow_ref = bf16[512,128]{1,0:T(8,128)(2,1)} fusion(f32[512,128]{1,0:T(8,128)} %param.17), kind=kLoop, calls=%fused_computation.26 | loop fusion | flops 131072 | bytes 393216 | tf_op jit(solution)/shard_map/convert_element_type | solution.py:307
  5.0 101.9 %shard_map.195 = (bf16[2,16,128,384]{3,2,1,0:T(8,128)(2,1)}, bf16[16,128,512]{2,1,0:T(8,128)(2,1)}, bf16[16,512,128]{2,1,0:T(8,128)(2,1)}, f32[16,24,512]{2,1,0:T(8,128)}, f32[16,32,384]{2,1,0:T(8,128)}) custom-call(bf16[1024,2048]{1,0:T(8,128)(2,1)} %x_hbm.1, bf16[1024,512]{1,0:T(8,128)(2,1)} %v_hbm.1, bf16[1024,512]{1,0:T(8,128)(2,1)} %m_hbm.1, ...), custom_call_target="tpu_custom_call" | custom-call | tf_op jit(solution)/shard_map/pallas_call | solution.py:253
  106.9 0.0 copy-start.9
  106.9 2.0 %multiply_reduce_fusion.1 = f32[]{:T(128)} fusion(f32[16,24,512]{2,1,0:T(8,128)} %get-tuple-element.15), kind=kLoop, calls=%fused_computation.21 | loop fusion | flops 393215 | bytes 786436 | tf_op jit(solution)/shard_map/reduce_sum | solution.py:310
  108.9 1.9 %multiply_reduce_fusion = f32[]{:T(128)} fusion(f32[16,32,384]{2,1,0:T(8,128)} %get-tuple-element.16), kind=kLoop, calls=%fused_computation.20 | loop fusion | flops 393215 | bytes 786436 | tf_op jit(solution)/shard_map/reduce_sum | solution.py:310
  112.1 3.2 %psum.7 = f32[]{:T(128)} all-reduce(f32[]{:T(128)S(6)} %add.41), channel_id=1, replica_groups=mesh['fs'=16,'tp'=2] {'tp'}, use_global_device_ids=true, to_apply=%region_2.0 | all-reduce | flops 1 | bytes 8 | tf_op jit(solution)/shard_map/psum | solution.py:310
  116.0 1.2 broadcast_multiply_fusion.1
  117.2 1.7 %subtract_convert_fusion.2 = (bf16[384,512]{1,0:T(8,128)(2,1)S(1)}, f32[384,512]{1,0:T(8,128)S(1)}, f32[384,512]{1,0:T(8,128)S(1)}) fusion(f32[16,24,512]{2,1,0:T(8,128)S(1)} %broadcast_multiply_fusion.1, f32[384,512]{1,0:T(8,128)} %param.21, f32[384,512]{1,0:T(8,128)} %param.20), kind=kLoop, calls=%fused_computation.18 | loop fusion | flops 2555904 | bytes 4325376 | tf_op jit(solution)/shard_map/convert_element_type | solution.py:281
  118.9 0.0 copy-start.3
  118.9 0.0 copy-start.4
  119.0 0.0 copy-done.9
  119.0 0.3 fusion.14
  119.3 1.0 multiply_subtract_fusion.1
  120.3 0.8 copy.28
  121.2 0.0 copy-start.5
  121.2 2.4 %log_multiply_fusion = f32[16,128,512]{2,1,0:T(8,128)S(1)} fusion(bf16[16,128,512]{2,1,0:T(8,128)(2,1)} %get-tuple-element.17), kind=kLoop, calls=%fused_computation.4 | loop fusion | flops 2097152 | bytes 6291456 | tf_op jit(solution)/shard_map/mul | solution.py:327
  123.6 0.1 copy-done.5
  123.7 0.5 fusion.20
  124.2 0.0 copy-done.3
  124.2 0.0 copy-done.4
  124.2 1.3 fusion.12
  125.5 0.0 copy-start.8
  125.5 0.0 copy-start.6
  125.5 2.6 %fusion = bf16[2048,512]{1,0:T(8,128)(2,1)} fusion(f32[16,128,512]{2,1,0:T(8,128)S(1)} %log_multiply_fusion, f32[2048,512]{1,0:T(8,128)S(1)} %fusion.12, bf16[2048,384]{1,0:T(8,128)(2,1)S(1)} %bitcast.38, bf16[384,512]{1,0:T(8,128)(2,1)S(1)} %get-tuple-element.43), kind=kOutput, calls=%fused_computation.1 | convolution fusion | flops 809500672 | bytes 12451840 | tf_op jit(solution)/shard_map/dot_general | solution.py:284
  128.2 0.0 copy-done.8
  128.2 0.8 copy.29
  129.0 0.0 copy-done.6
  129.0 0.1 broadcast_multiply_fusion
  129.1 0.0 copy-start.7
  129.1 1.9 %subtract_convert_fusion.1 = (bf16[512,384]{1,0:T(8,128)(2,1)S(1)}, f32[512,384]{1,0:T(8,128)S(1)}, f32[512,384]{1,0:T(8,128)S(1)}) fusion(f32[16,32,384]{2,1,0:T(8,128)S(1)} %broadcast_multiply_fusion, f32[512,384]{1,0:T(8,128)} %param.23, f32[512,384]{1,0:T(8,128)} %param.22), kind=kLoop, calls=%fused_computation.16 | loop fusion | flops 2555904 | bytes 4325376 | tf_op jit(solution)/shard_map/convert_element_type | solution.py:281
  131.0 0.0 copy-start.1
  131.0 0.0 copy-start.2
  131.0 1.3 fusion.10
  132.3 2.1 %multiply_subtract_fusion = (f32[512,128]{1,0:T(8,128)}, f32[512,128]{1,0:T(8,128)}) fusion(f32[512,128]{1,0:T(8,128)} %param.17, f32[512,128]{1,0:T(8,128)S(1)} %fusion.10, bf16[512,384]{1,0:T(8,128)(2,1)S(1)} %get-tuple-element.40, bf16[128,384]{1,0:T(8,128)(2,1)} %ob_ref.1), kind=kOutput, calls=%fused_computation.24 | convolution fusion | flops 50528256 | bytes 1540096 | tf_op jit(solution)/shard_map/dot_general | solution.py:283
  134.3 0.0 copy-done.7
  134.3 2.6 %multiply_bitcast_fusion = f32[512,16,128]{2,0,1:T(8,128)} fusion(bf16[16,512,128]{2,1,0:T(8,128)(2,1)S(1)} %copy-done.7), kind=kLoop, calls=%fused_computation.3 | loop fusion | flops 2097152 | bytes 6291456 | tf_op jit(solution)/shard_map/mul | solution.py:329
  136.9 5.4 %copy.26 = f32[512,16,128]{0,2,1:T(8,128)} copy(f32[512,16,128]{2,0,1:T(8,128)} %multiply_bitcast_fusion) | data formatting | bytes 8388608 | tf_op jit(solution)/shard_map/mul | solution.py:329
  142.3 5.4 %copy.27 = f32[512,2048]{1,0:T(8,128)} copy(f32[512,2048]{0,1:T(8,128)} %bitcast.39) | data formatting | bytes 8388608 | tf_op jit(solution)/shard_map/mul | solution.py:329
  147.7 0.0 copy-done.1
  147.7 0.0 copy-done.2
  147.7 0.0 copy-start
  147.7 1.3 fusion.8
  149.0 0.9 copy-done
  149.9 2.7 %subtract_convert_fusion = bf16[512,2048]{1,0:T(8,128)(2,1)} fusion(f32[512,2048]{1,0:T(8,128)S(1)} %copy-done, f32[512,2048]{1,0:T(8,128)S(1)} %fusion.8, bf16[512,384]{1,0:T(8,128)(2,1)S(1)} %get-tuple-element.40, bf16[2048,384]{1,0:T(8,128)(2,1)S(1)} %bitcast.41), kind=kOutput, calls=%fused_computation.2 | convolution fusion | flops 809500672 | bytes 12451840 | tf_op jit(solution)/shard_map/dot_general | solution.py:283
Async XLA Ops:
  106.9 12.0 %copy-start.9 = (bf16[128,384]{1,0:T(8,128)(2,1)S(1)}, bf16[128,384]{1,0:T(8,128)(2,1)}, u32[]{:S(2)}) copy-start(bf16[128,384]{1,0:T(8,128)(2,1)} %vb_ref.1) | copy-start | bytes 294916
  118.9 5.3 %copy-start.3 = (f32[384,512]{1,0:T(8,128)}, f32[384,512]{1,0:T(8,128)S(1)}, u32[]{:S(2)}) copy-start(f32[384,512]{1,0:T(8,128)S(1)} %get-tuple-element.44) | copy-start | bytes 2359300
  118.9 5.3 %copy-start.4 = (f32[384,512]{1,0:T(8,128)}, f32[384,512]{1,0:T(8,128)S(1)}, u32[]{:S(2)}) copy-start(f32[384,512]{1,0:T(8,128)S(1)} %get-tuple-element.45) | copy-start | bytes 2359300
  121.2 2.5 %copy-start.5 = (bf16[2,16,128,384]{3,2,1,0:T(8,128)(2,1)S(1)}, bf16[2,16,128,384]{3,2,1,0:T(8,128)(2,1)}, u32[]{:S(2)}) copy-start(bf16[2,16,128,384]{3,2,1,0:T(8,128)(2,1)} %get-tuple-element.18) | copy-start | bytes 9437188
  125.5 2.7 %copy-start.8 = (f32[128,512]{0,1:T(8,128)S(1)}, f32[128,512]{0,1:T(8,128)}, u32[]{:S(2)}) copy-start(f32[128,512]{0,1:T(8,128)} %get-tuple-element.49) | copy-start | bytes 786436
  125.5 3.5 %copy-start.6 = (f32[16,32,384]{2,1,0:T(8,128)S(1)}, f32[16,32,384]{2,1,0:T(8,128)}, u32[]{:S(2)}) copy-start(f32[16,32,384]{2,1,0:T(8,128)} %get-tuple-element.16) | copy-start | bytes 2359300
  129.1 5.3 %copy-start.7 = (bf16[16,512,128]{2,1,0:T(8,128)(2,1)S(1)}, bf16[16,512,128]{2,1,0:T(8,128)(2,1)}, u32[]{:S(2)}) copy-start(bf16[16,512,128]{2,1,0:T(8,128)(2,1)} %get-tuple-element.19) | copy-start | bytes 6291460
  131.0 16.7 %copy-start.1 = (f32[512,384]{1,0:T(8,128)}, f32[512,384]{1,0:T(8,128)S(1)}, u32[]{:S(2)}) copy-start(f32[512,384]{1,0:T(8,128)S(1)} %get-tuple-element.41) | copy-start | bytes 2359300
  131.0 16.7 %copy-start.2 = (f32[512,384]{1,0:T(8,128)}, f32[512,384]{1,0:T(8,128)S(1)}, u32[]{:S(2)}) copy-start(f32[512,384]{1,0:T(8,128)S(1)} %get-tuple-element.42) | copy-start | bytes 2359300
  147.7 2.2 %copy-start = (f32[512,2048]{1,0:T(8,128)S(1)}, f32[512,2048]{1,0:T(8,128)}, u32[]{:S(2)}) copy-start(f32[512,2048]{1,0:T(8,128)} %copy.27) | copy-start | bytes 12582916

commit v2 on v1

--- a/solution.py
+++ b/solution.py
@@ -11,6 +11,8 @@
 MESH = pl.DeviceIdType.MESH
 VALUE_RATE = 125.0 / 0.125
 OUTPUT_RATE = 125.0 / 0.1875
+LOW_RATE = 124.0
+BLOCK_LANES = 256
 TOKEN_TILE = 256
 
 
@@ -107,16 +109,16 @@
 
 
 def exchange(n, scaling, x_hbm, v_hbm, m_hbm, o_hbm, vb_ref, ob_ref, vw_ref, ow_ref,
-             bases, wv, wo, low_v, low_o,
-             x_ref, v_ref, m_ref, o_ref, acc_v, acc_o, part_v, part_o, got_v, got_o,
-             load_sem, own_sem, b_send, b_recv, c_send, c_recv, w_send, w_recv, l_send, l_recv, r_send, r_recv):
+             bases, wv, wo, low_v, low_o, sums,
+             vw32, ow32, x_ref, v_ref, m_ref, o_ref, acc_v, acc_o, part_v, part_o, got_v, got_o,
+             load_sem, own_sem, b_send, b_recv, c_send, c_recv, w_send, w_recv, l_send, l_recv, r_send, r_recv, q_send, q_recv):
     p = Place(n)
     a = p.sizes[0]
     par, me = p.par, p.me
     loads = [pltpu.make_async_copy(s, d, load_sem.at[i]) for i, (s, d) in enumerate(
-        ((x_hbm, x_ref), (v_hbm, v_ref), (o_hbm, o_ref), (m_hbm, m_ref)))]
+        ((vw_ref, vw32), (ow_ref, ow32), (x_hbm, x_ref), (v_hbm, v_ref), (o_hbm, o_ref), (m_hbm, m_ref)))]
     own = [pltpu.make_async_copy(s, d, own_sem.at[i]) for i, (s, d) in enumerate(
-        ((vb_ref, bases.at[0, me]), (ob_ref, bases.at[1, me]), (vw_ref, wv.at[me]), (ow_ref, wo.at[me])))]
+        ((vb_ref, bases.at[0, me]), (ob_ref, bases.at[1, me])))]
     for c in own + loads:
         c.start()
     partner = p.core + 1 - 2 * par
@@ -124,8 +126,11 @@
     peers = [p.at(dz, 0, 0) for dz in range(1, a)] + [p.at(0, 1, 0), p.at(0, 0, 1)]
     for to in peers:
         pl.semaphore_signal(barrier, inc=1, device_id={"fs": to}, device_id_type=MESH)
-    pl.semaphore_signal(barrier, inc=1, device_id={"tp": partner}, device_id_type=MESH)
-    pl.semaphore_wait(barrier, len(peers) + 1)
+    cores = lax.axis_size("tp")
+    siblings = [lax.rem(p.core + d, cores) for d in range(1, cores)]
+    for to in siblings:
+        pl.semaphore_signal(barrier, inc=1, device_id={"tp": to}, device_id_type=MESH)
+    pl.semaphore_wait(barrier, len(peers) + len(siblings))
     for c in own:
         c.wait()
 
@@ -142,6 +147,10 @@
 
     gb = Gather(p, [lambda i: bases.at[par, i]], b_send, b_recv)
     gb.begin()
+    for c in loads[:2]:
+        c.wait()
+    wv[me] = jnp.exp2(VALUE_RATE * vw32[...]).astype(wv.dtype)
+    wo[me] = jnp.exp2(OUTPUT_RATE * ow32[...]).astype(wo.dtype)
     gb.stage_z(cross)
     gb.stage_s(cross)
     gb.stage_t(cross)
@@ -156,7 +165,7 @@
                     pltpu.make_async_remote_copy(
                         src_ref=ref, dst_ref=ref, send_sem=c_send.at[k], recv_sem=c_recv.at[k],
                         device_id={"tp": partner}, device_id_type=MESH).wait_recv()
-    for c in loads:
+    for c in loads[2:]:
         c.wait()
 
     depth, rank = bases.shape[2], bases.shape[3]
@@ -222,15 +231,46 @@
     gw.stage_z()
     for dz in range(1, a):
         take(me, 3 * a + dz)
-    low_v[me] = part_v[me]
-    low_o[me] = part_o[me]
+    mine_v, mine_o = part_v[me], part_o[me]
+
+    def one(reduce, value):
+        return reduce(reduce(value, axis=1, keepdims=True), axis=0, keepdims=True)
+
+    top = jnp.maximum(one(jnp.max, jnp.abs(mine_v)), one(jnp.max, jnp.abs(mine_o)))
+    top = jnp.maximum(top * 1.01, 1e-30).astype(low_v.dtype)
+    square = one(jnp.sum, mine_v * mine_v) + one(jnp.sum, mine_o * mine_o)
+    rate = LOW_RATE / top.astype(jnp.float32)
+    high = mine_v.shape[0]
+    pad = low_v.shape[1] - high
+    square_high, square_low = halves(square)
+    row = lax.broadcasted_iota(jnp.int32, (pad, mine_v.shape[1]), 0)
+    extra = jnp.where(row == 0, top.astype(jnp.float32), jnp.where(
+        row == 1, square_high.astype(jnp.float32), square_low.astype(jnp.float32)))
+    low_v[me] = jnp.concatenate([jnp.exp2(rate * mine_v), extra], axis=0).astype(low_v.dtype)
+    low_o[me] = jnp.exp2(rate * mine_o).astype(low_o.dtype)
     gl = Gather(p, [lambda i: low_v.at[i], lambda i: low_o.at[i]], l_send, l_recv)
     gl.begin()
     gl.stage_z()
     gl.stage_s()
     gl.stage_t()
+    total = jnp.zeros((1, 128), jnp.float32)
+    for i in range(n):
+        tail = low_v[i].astype(jnp.float32)
+        total += tail[high + 1:high + 2, :128] + tail[high + 2:high + 3, :128]
+    sums[p.core] = jnp.broadcast_to(total, sums.shape[1:])
+    for d, to in enumerate(siblings):
+        c = pltpu.make_async_remote_copy(
+            src_ref=sums.at[p.core], dst_ref=sums.at[p.core], send_sem=q_send.at[d], recv_sem=q_recv.at[d],
+            device_id={"tp": to}, device_id_type=MESH)
+        c.start()
+        sent.append(c)
     gw.stage_s()
     gw.stage_t()
+    for d in range(cores - 1):
+        ref = sums.at[lax.rem(p.core - d - 1 + cores, cores)]
+        pltpu.make_async_remote_copy(
+            src_ref=ref, dst_ref=ref, send_sem=q_send.at[d], recv_sem=q_recv.at[d],
+            device_id={"tp": partner}, device_id_type=MESH).wait_recv()
     for c in crossed + sent:
         c.wait_send()
     gb.finish()
@@ -238,12 +278,13 @@
     gl.finish()
 
 
-def low_and_weights(block_input, value_cotangent, mixed_output, output_cotangent, value_basis, output_basis, vw_code, ow_code):
+def low_and_weights(block_input, value_cotangent, mixed_output, output_cotangent, value_basis, output_basis, value_weight, output_weight):
     n = lax.axis_size("fs")
     depth, rank = value_basis.shape
     tokens, width = value_cotangent.shape
     wide = block_input.shape[1]
     a = split_fs(n)[0]
+    cores = lax.axis_size("tp")
     scaling = 1.0 / math.sqrt(tokens * n)
     f32, b16 = jnp.float32, jnp.bfloat16
     rv, ro = rank // n, width // n
@@ -254,34 +295,80 @@
         functools.partial(exchange, n, scaling),
         out_shape=(
             jax.ShapeDtypeStruct((2, n, depth, rank), b16),
-            jax.ShapeDtypeStruct((n,) + vw_code.shape, vw_code.dtype),
-            jax.ShapeDtypeStruct((n,) + ow_code.shape, ow_code.dtype),
-            jax.ShapeDtypeStruct((n, rv, width), f32),
-            jax.ShapeDtypeStruct((n, ro, rank), f32),
+            jax.ShapeDtypeStruct((n,) + value_weight.shape, b16),
+            jax.ShapeDtypeStruct((n,) + output_weight.shape, b16),
+            jax.ShapeDtypeStruct((n, (rv + 18) // 16 * 16, width), b16),
+            jax.ShapeDtypeStruct((n, ro, rank), b16),
+            jax.ShapeDtypeStruct((cores, 8, 128), f32),
         ),
-        in_specs=[hbm] * 4 + [vmem] * 4,
-        out_specs=[vmem] * 5,
+        in_specs=[hbm] * 4 + [hbm] * 4,
+        out_specs=[vmem] * 6,
         scratch_shapes=[
+            pltpu.VMEM(value_weight.shape, f32), pltpu.VMEM(output_weight.shape, f32),
             pltpu.VMEM((tokens, wide), b16), pltpu.VMEM((tokens, width), b16),
             pltpu.VMEM((tokens, width), b16), pltpu.VMEM((tokens, wide), b16),
             pltpu.VMEM((rank, width), f32), pltpu.VMEM((width, rank), f32),
             pltpu.VMEM((n, rv, width), f32), pltpu.VMEM((n, ro, rank), f32),
             pltpu.VMEM((4 * a, rv, width), f32), pltpu.VMEM((4 * a, ro, rank), f32),
-            dma((4,)), dma((4,)),
+            dma((6,)), dma((2,)),
             dma((1, 4 * a)), dma((1, 4 * a)), dma((4 * a,)), dma((4 * a,)),
             dma((2, 4 * a)), dma((2, 4 * a)), dma((2, 4 * a)), dma((2, 4 * a)), dma((2, 4 * a)), dma((2, 4 * a)),
+            dma((cores,)), dma((cores,)),
         ],
         compiler_params=pltpu.CompilerParams(
             collective_id=0, has_side_effects=True, vmem_limit_bytes=60 * 1024 * 1024),
-    )(block_input, value_cotangent, mixed_output, output_cotangent, value_basis, output_basis, vw_code, ow_code)
-
-
-def stepped(norm, basis, flip):
-    high = norm.astype(jnp.bfloat16)
-    low = (norm - high.astype(jnp.float32)).astype(jnp.bfloat16)
-    if flip:
-        return sum(lax.dot_general(h, basis, (((1,), (1,)), ((), ())), preferred_element_type=jnp.float32) for h in (high, low))
-    return sum(jnp.dot(basis, h, preferred_element_type=jnp.float32) for h in (high, low))
+    )(block_input, value_cotangent, mixed_output, output_cotangent, value_basis, output_basis, value_weight, output_weight)
+
+
+def split_norm(norm, norms):
+    norms[0] = norm.astype(jnp.bfloat16)
+    norms[1] = (norm - norms[0].astype(jnp.float32)).astype(jnp.bfloat16)
+
+
+def value_steps(basis, norms):
+    return (jnp.dot(basis, norms[0], preferred_element_type=jnp.float32)
+            + jnp.dot(basis, norms[1], preferred_element_type=jnp.float32))
+
+
+def output_steps(basis, norms):
+    last = (((1,), (1,)), ((), ()))
+    return (lax.dot_general(norms[0], basis, last, preferred_element_type=jnp.float32)
+            + lax.dot_general(norms[1], basis, last, preferred_element_type=jnp.float32))
+
+
+def epilogue(entries, low_v, low_o, sums, vm, vs, om, os, vw, ow, vb, ob, bases, wv, wo,
+             v_next, v_copy, v_step, vm_next, vs_next, o_next, o_copy, o_step, om_next, os_next,
+             norms_v, norms_o):
+    @pl.when(pl.program_id(0) == 0)
+    def _():
+        n, high, high_o = low_v.shape[0], vm.shape[0] // low_v.shape[0], low_o.shape[1]
+        total = sums[0, :1, :1]
+        for i in range(1, sums.shape[0]):
+            total += sums[i, :1, :1]
+        clip = 1.0 / jnp.sqrt(1.0 + total / entries)
+        for i in range(n):
+            code = low_v[i].astype(jnp.float32)
+            rate = clip * code[high:high + 1, :1] * (1.0 / LOW_RATE)
+            for part, at, mean, square, mean_next, square_next in (
+                (code[:high], slice(i * high, (i + 1) * high), vm, vs, vm_next, vs_next),
+                (low_o[i].astype(jnp.float32), slice(i * high_o, (i + 1) * high_o), om, os, om_next, os_next),
+            ):
+                scaled = rate * jnp.log2(part)
+                mean_next[at] = 0.8 * mean[at] + 0.2 * scaled
+                square_next[at] = 0.9 * square[at] + 0.1 * scaled * scaled
+        split_norm(vm_next[...] / jnp.sqrt(vs_next[...] + 0.1), norms_v)
+        split_norm(om_next[...] / jnp.sqrt(os_next[...] + 0.1), norms_o)
+        v_step[...] = value_steps(vb[...], norms_v)
+        v_next[...] = vw[...] - 0.02 * v_step[...]
+        o_step[...] = output_steps(ob[...], norms_o)
+        o_next[...] = ow[...] - 0.02 * o_step[...]
+
+    count, rows, cols = wv.shape[0], wv.shape[1], wo.shape[2]
+    for k in range(count):
+        old = jnp.log2(wv[k].astype(jnp.float32)) * (1.0 / VALUE_RATE)
+        v_copy[k * rows:(k + 1) * rows, :] = (old - 0.02 * value_steps(bases[0, k], norms_v)).astype(v_copy.dtype)
+        old = jnp.log2(wo[k].astype(jnp.float32)) * (1.0 / OUTPUT_RATE)
+        o_copy[:, k * cols:(k + 1) * cols] = (old - 0.02 * output_steps(bases[1, k], norms_o)).astype(o_copy.dtype)
 
 
 def on_device(
@@ -298,48 +385,41 @@
     output_mean,
     output_square,
 ):
-    rank_size = value_basis.shape[1]
-    local_width = value_cotangent.shape[1]
-    wide = block_input.shape[1]
-    bases, wv, wo, value_low, output_low = low_and_weights(
+    n = lax.axis_size("fs")
+    depth, rank = value_basis.shape
+    width = value_cotangent.shape[1]
+    bases, wv, wo, low_v, low_o, sums = low_and_weights(
         block_input, value_cotangent, mixed_output, output_cotangent, value_basis, output_basis,
-        jnp.exp2(VALUE_RATE * value_weight).astype(jnp.bfloat16),
-        jnp.exp2(OUTPUT_RATE * output_weight).astype(jnp.bfloat16))
-    value_low = value_low.reshape(rank_size, local_width)
-    output_low = output_low.reshape(local_width, rank_size)
-    squares = lax.psum(jnp.sum(value_low * value_low) + jnp.sum(output_low * output_low), "tp")
-    entries = 2.0 * rank_size * local_width * lax.axis_size("tp")
-    clip_scale = 1.0 / jnp.sqrt(1.0 + squares / entries)
-    value_scaled = clip_scale * value_low
-    output_scaled = clip_scale * output_low
-    value_mean_next = 0.8 * value_mean + 0.2 * value_scaled
-    output_mean_next = 0.8 * output_mean + 0.2 * output_scaled
-    value_square_next = 0.9 * value_square + 0.1 * value_scaled * value_scaled
-    output_square_next = 0.9 * output_square + 0.1 * output_scaled * output_scaled
-    value_norm = value_mean_next / jnp.sqrt(value_square_next + 0.1)
-    output_norm = output_mean_next / jnp.sqrt(output_square_next + 0.1)
-    value_step = stepped(value_norm, value_basis, False)
-    output_step = stepped(output_norm, output_basis, True)
-    value_next = value_weight - 0.02 * value_step
-    output_next = output_weight - 0.02 * output_step
-    value_all = stepped(value_norm, bases[0].reshape(wide, rank_size), False)
-    output_all = stepped(output_norm, bases[1].reshape(wide, rank_size), True)
-    value_old = jnp.log2(wv.reshape(wide, local_width).astype(jnp.float32)) * (1.0 / VALUE_RATE)
-    value_copy = (value_old - 0.02 * value_all).astype(jnp.bfloat16)
-    output_old = jnp.log2(wo.transpose(1, 0, 2).reshape(local_width, wide).astype(jnp.float32)) * (1.0 / OUTPUT_RATE)
-    output_copy = (output_old - 0.02 * output_all).astype(jnp.bfloat16)
-    return (
-        value_next,
-        value_copy,
-        value_step,
-        value_mean_next,
-        value_square_next,
-        output_next,
-        output_copy,
-        output_step,
-        output_mean_next,
-        output_square_next,
-    )
+        value_weight, output_weight)
+    entries = 2.0 * rank * width * lax.axis_size("tp")
+    count = math.gcd(n, max(1, BLOCK_LANES // depth))
+
+    def full(array):
+        return pl.BlockSpec(array.shape, lambda i: (0,) * array.ndim)
+
+    f32, b16 = jnp.float32, jnp.bfloat16
+    small = [low_v, low_o, sums, value_mean, value_square, output_mean, output_square,
+             value_weight, output_weight, value_basis, output_basis]
+    v_row, v_small = jax.ShapeDtypeStruct((depth, width), f32), jax.ShapeDtypeStruct((rank, width), f32)
+    o_row, o_small = jax.ShapeDtypeStruct((width, depth), f32), jax.ShapeDtypeStruct((width, rank), f32)
+    v_all, o_all = jax.ShapeDtypeStruct((n * depth, width), b16), jax.ShapeDtypeStruct((width, n * depth), b16)
+    return pl.pallas_call(
+        functools.partial(epilogue, entries),
+        grid=(n // count,),
+        out_shape=(v_row, v_all, v_row, v_small, v_small, o_row, o_all, o_row, o_small, o_small),
+        in_specs=[full(array) for array in small] + [
+            pl.BlockSpec((2, count, depth, rank), lambda i: (0, i, 0, 0)),
+            pl.BlockSpec((count, depth, width), lambda i: (i, 0, 0)),
+            pl.BlockSpec((count, width, depth), lambda i: (i, 0, 0)),
+        ],
+        out_specs=[
+            full(v_row), pl.BlockSpec((count * depth, width), lambda i: (i, 0)), full(v_row), full(v_small), full(v_small),
+            full(o_row), pl.BlockSpec((width, count * depth), lambda i: (0, i)), full(o_row), full(o_small), full(o_small),
+        ],
+        scratch_shapes=[pltpu.VMEM((2, rank, width), b16), pltpu.VMEM((2, width, rank), b16)],
+        compiler_params=pltpu.CompilerParams(
+            dimension_semantics=("arbitrary",), vmem_limit_bytes=60 * 1024 * 1024),
+    )(*small, bases, wv, wo)
 
 
 def solution(mesh):

time: 154 us -> 114 us (0.74)
  other arithmetic: 17 us -> 0 us
  local copies, waits for them, and re-layouts: 15.1 us -> 0 us
  matrix products: 12.6 us -> 0 us
  Pallas kernels: 102 us -> 113 us
  blocking collectives: 3.15 us -> 0 us
  between operations: 2.81 us -> 0.65 us
    pallas_call x0 -> x1, Pallas kernels: none -> 14.3 us  [on_device(): pl.pallas_call(functools.partial(epilogue, entries), grid=(n // count,),...]
    dot_general x8 -> x0, matrix products: 12.6 us -> none  [the longest x4 7.34 us: stepped(): lax.dot_general(h, basis, (((1,), (1,)), ((), ())), preferred_element_typ...]
    mul x2 -> x0, local copies, waits for them, and re-layouts: 10.8 us -> none  [on_device(): jnp.log2(wo.transpose(1, 0, 2).reshape(local_width, wide).astype(jnp.floa...]
    convert_element_type x4 -> x0, other arithmetic: 6.91 us -> none  [the longest x2 3.61 us: stepped(): low = (norm - high.astype(jnp.float32)).astype(jnp.bfloat16)]
    mul x4 -> x0, other arithmetic: 6.22 us -> none  [the longest x1 2.55 us: on_device(): jnp.log2(wo.transpose(1, 0, 2).reshape(local_width, wide).astype(jnp.floa...]
    reduce_sum x2 -> x0, other arithmetic: 3.91 us -> none  [the longest x1 1.97 us: on_device(): jnp.sum(value_low * value_low) + jnp.sum(output_low * output_low)]
    unnamed x23 -> x0, local copies, waits for them, and re-layouts: 3.78 us -> none
    psum x1 -> x0, blocking collectives: 3.15 us -> none  [on_device(): lax.psum(jnp.sum(value_low * value_low) + jnp.sum(output_low * output_low...]
where the time goes in v2:
time: 114 us
  Pallas kernels  113 us (99%)
    pallas_call x1, Pallas kernels, low_and_weights(): pl.pallas_call(functools.partial(exchange, n, scaling), out_shape=(jax.Sh...  98.9 us
    pallas_call x1, Pallas kernels, on_device(): pl.pallas_call(functools.partial(epilogue, entries), grid=(n // count,),...  14.3 us

profile of v2, /device:TPU:0, one launch (start us, length us, event | category | flops | bytes accessed | tf_op | source)
XLA Modules:
  0.0 113.9 jit_solution(11904959542556592477)
XLA Ops:
  0.6 98.9 %shard_map.195 = (bf16[2,16,128,384]{3,2,1,0:T(8,128)(2,1)}, bf16[16,128,512]{2,1,0:T(8,128)(2,1)}, bf16[16,512,128]{2,1,0:T(8,128)(2,1)}, bf16[16,32,512]{2,1,0...) custom-call(bf16[1024,2048]{1,0:T(8,128)(2,1)} %x_hbm.1, bf16[1024,512]{1,0:T(8,128)(2,1)} %v_hbm.1, ...), custom_call_target="tpu_custom_call" | custom-call | tf_op jit(solution)/shard_map/pallas_call | solution.py:294
  99.5 14.3 %shard_map.196 = (f32[128,512]{1,0:T(8,128)}, bf16[2048,512]{1,0:T(8,128)(2,1)}, f32[128,512]{1,0:T(8,128)}, f32[384,512]{1,0:T(8,128)}, f32[384,512]{1,0:T(8,12...) custom-call(bf16[16,32,512]{2,1,0:T(8,128)(2,1)} %get-tuple-element., ...), custom_call_target="tpu_custom_call" | custom-call | tf_op jit(solution)/shard_map/pallas_call | solution.py:406

commit v3 on v2

--- a/solution.py
+++ b/solution.py
@@ -78,9 +78,15 @@
             self.go(j, self.p.at(-dz, ds, 0), self.p.at(0, 0, 1), 2 * self.a + dz * 2 + ds, self.rel(dz, ds, 1))
 
     def begin(self):
+        self.begin_z()
+        self.begin_st()
+
+    def begin_z(self):
         for dz in range(1, self.a):
             for j in range(len(self.slots)):
                 self.go(j, self.p.me, self.p.at(dz, 0, 0), dz, self.rel(dz, 0, 0))
+
+    def begin_st(self):
         self.to_s(0)
         self.to_t(0, 0)
 
@@ -152,10 +158,11 @@
     wv[me] = jnp.exp2(VALUE_RATE * vw32[...]).astype(wv.dtype)
     wo[me] = jnp.exp2(OUTPUT_RATE * ow32[...]).astype(wo.dtype)
     gb.stage_z(cross)
+    gw = Gather(p, [lambda i: wv.at[i], lambda i: wo.at[i]], w_send, w_recv)
+    gw.begin_z()
     gb.stage_s(cross)
     gb.stage_t(cross)
-    gw = Gather(p, [lambda i: wv.at[i], lambda i: wo.at[i]], w_send, w_recv)
-    gw.begin()
+    gw.begin_st()
     for dz in range(a):
         for ds in range(2):
             for dt in range(2):
@@ -220,6 +227,7 @@
     for dz in order:
         for ds in (1, 0):
             hand(p.at(dz, ds, 1), p.at(0, 0, 1), dz * 2 + ds)
+    gw.stage_z()
     for dz in order:
         take(p.at(dz, 1, 0), dz * 2 + 1)
         hand(p.at(dz, 1, 0), p.at(0, 1, 0), 2 * a + dz)
@@ -228,7 +236,6 @@
         take(p.at(dz, 0, 0), 2 * a + dz)
         if dz:
             hand(p.at(dz, 0, 0), p.at(dz, 0, 0), 3 * a + dz)
-    gw.stage_z()
     for dz in range(1, a):
         take(me, 3 * a + dz)
     mine_v, mine_o = part_v[me], part_o[me]
@@ -250,6 +257,7 @@
     low_o[me] = jnp.exp2(rate * mine_o).astype(low_o.dtype)
     gl = Gather(p, [lambda i: low_v.at[i], lambda i: low_o.at[i]], l_send, l_recv)
     gl.begin()
+    gw.stage_s()
     gl.stage_z()
     gl.stage_s()
     gl.stage_t()
@@ -264,7 +272,6 @@
             device_id={"tp": to}, device_id_type=MESH)
         c.start()
         sent.append(c)
-    gw.stage_s()
     gw.stage_t()
     for d in range(cores - 1):
         ref = sums.at[lax.rem(p.core - d - 1 + cores, cores)]

time: 114 us -> 113 us (level)
  the two profiles are of different devices: /device:TPU:0 before, /device:TPU:9 now
where the time goes in v3:
time: 113 us
  Pallas kernels  112 us (99%)
    pallas_call x1, Pallas kernels, low_and_weights(): pl.pallas_call(functools.partial(exchange, n, scaling), out_shape=(jax.Sh...  97.6 us
    pallas_call x1, Pallas kernels, on_device(): pl.pallas_call(functools.partial(epilogue, entries), grid=(n // count,),...  14.3 us

profile of v3, /device:TPU:9, one launch (start us, length us, event | category | flops | bytes accessed | tf_op | source)
XLA Modules:
  0.0 112.6 jit_solution(11443222307394364838)
XLA Ops:
  0.6 97.6 %shard_map.195 = (bf16[2,16,128,384]{3,2,1,0:T(8,128)(2,1)}, bf16[16,128,512]{2,1,0:T(8,128)(2,1)}, bf16[16,512,128]{2,1,0:T(8,128)(2,1)}, bf16[16,32,512]{2,1,0...) custom-call(bf16[1024,2048]{1,0:T(8,128)(2,1)} %x_hbm.1, bf16[1024,512]{1,0:T(8,128)(2,1)} %v_hbm.1, ...), custom_call_target="tpu_custom_call" | custom-call | tf_op jit(solution)/shard_map/pallas_call | solution.py:301
  98.3 14.3 %shard_map.196 = (f32[128,512]{1,0:T(8,128)}, bf16[2048,512]{1,0:T(8,128)(2,1)}, f32[128,512]{1,0:T(8,128)}, f32[384,512]{1,0:T(8,128)}, f32[384,512]{1,0:T(8,12...) custom-call(bf16[16,32,512]{2,1,0:T(8,128)(2,1)} %get-tuple-element., ...), custom_call_target="tpu_custom_call" | custom-call | tf_op jit(solution)/shard_map/pallas_call | solution.py:413
